TPU v7x, 32 devices: a whole 2x2x4 slice. The times are simulated.
32 devices in a mesh: grp: 2 (over x), tp: 4 (over y, core), dp: 4 (over z).
Axes of the slice: x: 2, y: 2, z: 4, core: 2. Of those that a mesh axis runs over, the one named last changes fastest.
Arguments:
- tokens: bfloat16 [512, 2048], P(('grp', 'tp'), 'dp'), parts along dimension 0, may hold values from -25 to 25
- state: float32 [2, 512, 16, 128, 128], P(None, ('grp', 'dp'), 'tp'), parts along dimension 1, may hold values from -1 to 1
- lengths: int32 [512], P(('grp', 'dp')), parts along dimension 0, may hold values from 1 to 4096, 131072 in all
- norm_gain: bfloat16 [2, 2048], P(None, 'dp'), may hold values from 0.099609375 to 1.8984375
- w_query: bfloat16 [2, 2048, 2048], P(None, 'dp', 'tp'), may hold values from -0.125 to 0.125
- w_forget: bfloat16 [2, 2048, 2048], P(None, 'dp', 'tp'), may hold values from -0.125 to 0.125
- w_input: bfloat16 [2, 2048, 2048], P(None, 'dp', 'tp'), may hold values from -0.125 to 0.125
- w_gate: bfloat16 [2, 2048, 2048], P(None, 'dp', 'tp'), may hold values from -0.125 to 0.125
- w_out: bfloat16 [2, 2048, 2048], P(None, 'tp', 'dp'), may hold values from -0.125 to 0.125
- bound_logit: float32 [2, 2048], P(None, 'tp'), may hold values from -3 to 5
- pace: float32 [2, 2048], P(None, 'tp'), may hold values from 0.6 to 2
- head_gain: float32 [2, 128], replicated, may hold values from 0.4 to 2.5
Outputs:
- mixed: float32 [512, 2048], P(('grp', 'tp'), 'dp'), parts along dimension 0
- new_state: float32 [2, 512, 16, 128, 128], P(None, ('grp', 'dp'), 'tp'), parts along dimension 1
There are 2 independent parts, one for each index of `grp`. A program takes and returns all parts, laid end to end along the dimension named above; an argument that names none is the same for every part. Nothing has to cross between parts.
All inputs are finite; a program needn't handle non-finite values. No bound on the sum of `lengths` on one device may be relied on, other than what follows from the above.
Results may differ from a plain program's by a relative error of at most 0.0083.
Values may be sent and summed in bfloat16 or wider, within the bound.
A program may use at most 192 MiB of HBM per device.

v0:
```python
import jax
import jax.numpy as jnp
from jax import lax
from jax.sharding import PartitionSpec as P

D = 2048
LENGTH_MEAN = 512
epsilon = 1e-06


def advance(prior, query, forget_in, value, gate, lower, pace_row, log_len, gain_row):
    count, width = query.shape
    size = prior.shape[-1]
    heads = width // size
    pre = forget_in - pace_row[None, :] * log_len[:, None]
    forget = lower[None, :] + (1.0 - lower[None, :]) * jax.nn.sigmoid(pre)
    key = (1.0 - lower[None, :]) * jax.nn.sigmoid(-pre)
    forget = forget.reshape(count, heads, size)
    key = key.reshape(count, heads, size)
    values = value.reshape(count, heads, size)
    updated = forget[..., None] * prior + key[..., None] * values[:, :, None, :]
    readout = jnp.einsum(
        "bhk,bhkv->bhv", query.reshape(count, heads, size), updated, precision=lax.Precision.HIGHEST
    )
    normed = readout * lax.rsqrt(jnp.mean(readout * readout, axis=-1, keepdims=True) + epsilon)
    gates = gate.reshape(count, heads, size)
    normed = normed * gain_row[None, None, :] * jax.nn.silu(gates)
    return (updated, normed.reshape(count, width).astype(jnp.bfloat16))


def shards(
    tokens,
    state,
    lengths,
    norm_gain,
    w_query,
    w_forget,
    w_input,
    w_gate,
    w_out,
    bound_logit,
    pace,
    head_gain,
):
    current = tokens
    log_len = jnp.log(lengths.astype(jnp.float32) / LENGTH_MEAN)
    own_count = state.shape[1]
    states = []
    result = None
    for block in range(2):
        whole = lax.all_gather(current, "tp", axis=0, tiled=True)
        whole_wide = whole.astype(jnp.float32)
        partial_sq = jnp.sum(whole_wide * whole_wide, axis=1)
        squares_all = lax.psum(partial_sq, "dp")
        squares = lax.dynamic_slice_in_dim(
            squares_all, lax.axis_index("dp") * own_count, own_count, 0
        )
        gained = (whole_wide * norm_gain[block].astype(jnp.float32)[None, :]).astype(jnp.bfloat16)
        terms = tuple(
            (
                jnp.dot(gained, weight[block], preferred_element_type=jnp.float32)
                for weight in (w_query, w_forget, w_input, w_gate)
            )
        )
        sums = lax.psum_scatter(terms, "dp", scatter_dimension=0, tiled=True)
        scale = lax.rsqrt(squares / D + epsilon)
        made = [scale[:, None] * total for total in sums]
        lower = jax.nn.sigmoid(bound_logit[block])
        updated, normed = advance(
            state[block],
            made[0],
            made[1],
            made[2],
            made[3],
            lower,
            pace[block],
            log_len,
            head_gain[block],
        )
        states.append(updated)
        gathered = lax.all_gather(normed, "dp", axis=0, tiled=True)
        out_weight = w_out[block]
        branch = lax.psum_scatter(
            jnp.dot(gathered, out_weight, preferred_element_type=jnp.float32),
            "tp",
            scatter_dimension=0,
            tiled=True,
        )
        if block == 0:
            current = (current.astype(jnp.float32) + branch).astype(jnp.bfloat16)
        else:
            result = current.astype(jnp.float32) + branch
    return (result, jnp.stack(states))


def solution(mesh):
    in_specs = (
        P(("grp", "tp"), "dp"),
        P(None, ("grp", "dp"), "tp", None, None),
        P(("grp", "dp")),
        P(None, "dp"),
        P(None, "dp", "tp"),
        P(None, "dp", "tp"),
        P(None, "dp", "tp"),
        P(None, "dp", "tp"),
        P(None, "tp", "dp"),
        P(None, "tp"),
        P(None, "tp"),
        P(),
    )
    out_specs = (P(("grp", "tp"), "dp"), P(None, ("grp", "dp"), "tp", None, None))
    return jax.shard_map(shards, mesh=mesh, in_specs=in_specs, out_specs=out_specs, check_vma=False)
```

profile of v0, /device:TPU:0, one launch (start us, length us, event | category | flops | bytes accessed | tf_op | source)
XLA Modules:
  0.0 361.6 jit_solution(16375477499638168452)
XLA Ops:
  7.2 0.8 slice_convert_fusion
  8.0 7.4 %all_gather.12 = bf16[256,512]{1,0:T(8,128)(2,1)S(1)} all-gather(bf16[64,512]{1,0:T(8,128)(2,1)} %param.12), channel_id=1, replica_groups=mesh['grp'=2,'tp'=4,'dp'=4] {'tp'}, dimensions={0}, use_global_device_ids=true | all-gather | bytes 327680 | tf_op jit(solution)/shard_map/all_gather | solution.py:51
  15.4 2.1 fusion.36
  17.6 2.1 fusion.34
  19.8 2.2 fusion.32
  22.1 2.2 fusion.38
  24.3 0.1 fusion.16
  24.5 12.0 %psum.14 = f32[256]{0:T(256)S(1)} all-reduce(f32[256]{0:T(256)S(1)} %fusion.16), channel_id=1, replica_groups=mesh['grp'=2,'tp'=4,'dp'=4] {'dp'}, use_global_device_ids=true, to_apply=%region_1.0 | all-reduce | flops 256 | bytes 2048 | tf_op jit(solution)/shard_map/psum | solution.py:54
  36.4 0.1 add_rsqrt_fusion.3
  36.5 0.7 multiply_log_fusion
  37.2 1.3 slice_bitcast_fusion
  38.5 0.8 fusion.62
  39.3 0.8 broadcast_subtract_fusion
  40.1 0.8 reduce-scatter.13.cloned.1.call-done
  40.9 22.4 %reduce-scatter.15.cloned.1.call-done = f32[64,512]{1,0:T(8,128)} async-done(((f32[256,512]{1,0:T(8,128)}), f32[64,512]{1,0:T(8,128)}) %reduce-scatter.15.cloned.1.call-update) | async-done | bytes 131088 | tf_op jit(solution)/shard_map/reduce_scatter | solution.py:65
  63.4 22.4 %reduce-scatter.17.cloned.1.call-done = f32[64,512]{1,0:T(8,128)} async-done(((f32[256,512]{1,0:T(8,128)}), f32[64,512]{1,0:T(8,128)}) %reduce-scatter.17.cloned.1.call-update) | async-done | bytes 131088 | tf_op jit(solution)/shard_map/reduce_scatter | solution.py:65
  85.8 22.2 %reduce-scatter.11.cloned.1.call-done = f32[64,512]{1,0:T(8,128)} async-done(((f32[256,512]{1,0:T(8,128)}), f32[64,512]{1,0:T(8,128)}) %reduce-scatter.11.cloned.1.call-update) | async-done | bytes 131088 | tf_op jit(solution)/shard_map/reduce_scatter | solution.py:65
  108.0 1.2 multiply_add_fusion.3
  109.5 0.7 reshape.56
  110.2 0.7 reshape.61
  110.9 22.7 %fusion.4 = f32[64,4,1,128]{3,2,1,0:T(1,128)S(1)} fusion(f32[64,4,128,1]{2,3,1,0:T(1,128)} %bitcast.79, f32[2,64,4,128,128]{4,3,2,1,0:T(8,128)} %param.13, f32[64,4,128]{2,1,0:T(4,128)S(1)} %mul.316, f32[64,4,128]{2,1,0:T(4,128)S(1)} %mul.313, f32[64,4,128]{2,1,0:T(4,128)S(1)} %mul.309), kind=kOutput, calls=%fused_computation.6 | convolution fusion | flops 62914560 | bytes 17432576 | tf_op jit(solution)/shard_map/bhk,bhkv->bhv/dot_general | solution.py:22
  133.6 0.1 multiply_reduce_fusion.1
  133.8 0.1 fusion.61
  134.0 13.8 %all_gather.13 = bf16[256,512]{1,0:T(8,128)(2,1)S(1)} all-gather(bf16[64,512]{1,0:T(8,128)(2,1)S(1)} %bitcast.74), channel_id=1, replica_groups=mesh['grp'=2,'tp'=4,'dp'=4] {'dp'}, dimensions={0}, use_global_device_ids=true | all-gather | bytes 327680 | tf_op jit(solution)/shard_map/all_gather | solution.py:81
  147.8 2.1 fusion.30
  150.0 19.9 %reduce-scatter.19.cloned.1.call-done = f32[64,512]{1,0:T(8,128)} async-done(((f32[256,512]{1,0:T(8,128)}), f32[64,512]{1,0:T(8,128)}) %reduce-scatter.19.cloned.1.call-update) | async-done | bytes 131088 | tf_op jit(solution)/shard_map/reduce_scatter | solution.py:83
  169.9 0.9 add_convert_fusion
  170.9 5.8 %all_gather.14 = bf16[256,512]{1,0:T(8,128)(2,1)S(1)} all-gather(bf16[64,512]{1,0:T(8,128)(2,1)S(1)} %add_convert_fusion), channel_id=1, replica_groups=mesh['grp'=2,'tp'=4,'dp'=4] {'tp'}, dimensions={0}, use_global_device_ids=true | all-gather | bytes 327680 | tf_op jit(solution)/shard_map/all_gather | solution.py:51
  176.7 1.1 fusion.26
  177.8 1.1 fusion.24
  179.0 1.1 fusion.22
  180.2 2.2 fusion.28
  182.4 0.1 fusion.18
  182.6 11.7 %psum.15 = f32[256]{0:T(256)S(1)} all-reduce(f32[256]{0:T(256)S(1)} %fusion.18), channel_id=1, replica_groups=mesh['grp'=2,'tp'=4,'dp'=4] {'dp'}, use_global_device_ids=true, to_apply=%region_9.10 | all-reduce | flops 256 | bytes 2048 | tf_op jit(solution)/shard_map/psum | solution.py:54
  194.3 0.1 add_rsqrt_fusion.2
  194.4 5.5 %reduce-scatter.23.cloned.1.call-done = f32[64,512]{1,0:T(8,128)} async-done(((f32[256,512]{1,0:T(8,128)}), f32[64,512]{1,0:T(8,128)}) %reduce-scatter.23.cloned.1.call-update) | async-done | bytes 131088 | tf_op jit(solution)/shard_map/reduce_scatter | solution.py:65
  199.9 22.4 %reduce-scatter.25.cloned.1.call-done = f32[64,512]{1,0:T(8,128)} async-done(((f32[256,512]{1,0:T(8,128)}), f32[64,512]{1,0:T(8,128)}) %reduce-scatter.25.cloned.1.call-update) | async-done | bytes 131088 | tf_op jit(solution)/shard_map/reduce_scatter | solution.py:65
  222.3 22.4 %reduce-scatter.27.cloned.1.call-done = f32[64,512]{1,0:T(8,128)} async-done(((f32[256,512]{1,0:T(8,128)}), f32[64,512]{1,0:T(8,128)}) %reduce-scatter.27.cloned.1.call-update) | async-done | bytes 131088 | tf_op jit(solution)/shard_map/reduce_scatter | solution.py:65
  244.7 22.4 %reduce-scatter.21.cloned.1.call-done = f32[64,512]{1,0:T(8,128)} async-done(((f32[256,512]{1,0:T(8,128)}), f32[64,512]{1,0:T(8,128)}) %reduce-scatter.21.cloned.1.call-update) | async-done | bytes 131088 | tf_op jit(solution)/shard_map/reduce_scatter | solution.py:65
  267.1 1.2 multiply_add_fusion.2
  268.6 23.2 %multiply_add_fusion.1 = (f32[1,64,4,128,128]{4,3,2,1,0:T(8,128)}, f32[1,64,4,128,128]{4,3,2,1,0:T(8,128)}) fusion(f32[2,64,4,128,128]{4,3,2,1,0:T(8,128)} %param.13, f32[64,4,128]{2,1,0:T(4,128)} %copy-done.6, f32[64,4,128]{2,1,0:T(4,128)} %copy-done.5, f32[64,4,128]{2,1,0:T(4,128)} %copy-done.4, f32[64,4,128]{2,1,0:T(4,128)S(1)} %mul.349, ...), kind=kLoop, calls=%fused_computation.8 | loop fusion | flops 25165824 | bytes 67895296 | tf_op jit(solution)/shard_map/add | solution.py:21
  291.8 22.6 %fusion.1 = f32[64,4,1,128]{3,2,1,0:T(1,128)S(1)} fusion(f32[64,4,128,1]{2,3,1,0:T(1,128)S(1)} %bitcast.78, f32[2,64,4,128,128]{4,3,2,1,0:T(8,128)} %param.13, f32[64,4,128]{2,1,0:T(4,128)S(1)} %mul.349, f32[64,4,128]{2,1,0:T(4,128)S(1)} %mul.346, f32[64,4,128]{2,1,0:T(4,128)S(1)} %mul.342), kind=kOutput, calls=%fused_computation.3 | convolution fusion | flops 62914560 | bytes 17432576 | tf_op jit(solution)/shard_map/bhk,bhkv->bhv/dot_general | solution.py:22
  314.4 0.1 multiply_reduce_fusion
  314.6 0.1 fusion.60
  314.8 13.8 %all_gather.15 = bf16[256,512]{1,0:T(8,128)(2,1)S(1)} all-gather(bf16[64,512]{1,0:T(8,128)(2,1)S(1)} %bitcast.75), channel_id=1, replica_groups=mesh['grp'=2,'tp'=4,'dp'=4] {'dp'}, dimensions={0}, use_global_device_ids=true | all-gather | bytes 327680 | tf_op jit(solution)/shard_map/all_gather | solution.py:81
  328.6 1.1 fusion.20
  329.7 23.4 %pad_maximum_fusion = f32[2,64,4,128,128]{4,3,2,1,0:T(8,128)} fusion(f32[1,64,4,128,128]{4,3,2,1,0:T(8,128)} %get-tuple-element.7, f32[1,64,4,128,128]{4,3,2,1,0:T(8,128)} %get-tuple-element.6), kind=kLoop, calls=%fused_computation | loop fusion | flops 8388608 | bytes 67108864 | tf_op jit(solution)/shard_map/stack | solution.py:93
  353.1 1.6 convert_add_fusion
  (55 shorter events, 1.1 us)
Async XLA Ops:
  7.2 33.7 %reduce-scatter.13.cloned.1.call-start = ((), (), s32[]{:S(2)}) async-start(), calls=%async_computation.11 | async-start | bytes 655360 | tf_op jit(solution)/shard_map/reduce_scatter | solution.py:65
  17.6 45.8 %reduce-scatter.15.cloned.1.call-start = ((), (), s32[]{:S(2)}) async-start(), calls=%async_computation.12 | async-start | bytes 655360 | tf_op jit(solution)/shard_map/reduce_scatter | solution.py:65
  19.8 66.0 %reduce-scatter.17.cloned.1.call-start = ((), (), s32[]{:S(2)}) async-start(), calls=%async_computation.13 | async-start | bytes 655360 | tf_op jit(solution)/shard_map/reduce_scatter | solution.py:65
  22.0 86.0 %reduce-scatter.11.cloned.1.call-start = ((), (), s32[]{:S(2)}) async-start(), calls=%async_computation.10 | async-start | bytes 655360 | tf_op jit(solution)/shard_map/reduce_scatter | solution.py:65
  24.3 145.7 %reduce-scatter.19.cloned.1.call-start = ((), (), s32[]{:S(2)}) async-start(), calls=%async_computation.14 | async-start | bytes 655360 | tf_op jit(solution)/shard_map/reduce_scatter | solution.py:83
  37.2 73.7 %copy-start.8 = (f32[64]{0:T(128)}, f32[64]{0:T(128)S(1)}, u32[]{:S(2)}) copy-start(f32[64]{0:T(128)S(1)} %multiply_log_fusion) | copy-start | bytes 772
  109.3 24.6 %copy-start.4 = (f32[64,4,128]{2,1,0:T(4,128)}, f32[64,4,128]{2,1,0:T(4,128)S(1)}, u32[]{:S(2)}) copy-start(f32[64,4,128]{2,1,0:T(4,128)S(1)} %mul.309) | copy-start | bytes 393220
  109.4 24.6 %copy-start.5 = (f32[64,4,128]{2,1,0:T(4,128)}, f32[64,4,128]{2,1,0:T(4,128)S(1)}, u32[]{:S(2)}) copy-start(f32[64,4,128]{2,1,0:T(4,128)S(1)} %mul.313) | copy-start | bytes 393220
  109.5 40.5 %copy-start.6 = (f32[64,4,128]{2,1,0:T(4,128)}, f32[64,4,128]{2,1,0:T(4,128)S(1)}, u32[]{:S(2)}) copy-start(f32[64,4,128]{2,1,0:T(4,128)S(1)} %mul.316) | copy-start | bytes 393220
  110.9 22.9 %copy-start.7 = (f32[64,4,128]{2,1,0:T(4,128)S(1)}, f32[64,4,128]{2,1,0:T(4,128)}, u32[]{:S(2)}) copy-start(f32[64,4,128]{2,1,0:T(4,128)} %reshape.56) | copy-start | bytes 393220
  110.9 22.9 %copy-start.10 = (f32[128]{0:T(128)S(1)}, f32[128]{0:T(128)}, u32[]{:S(2)}) copy-start(f32[128]{0:T(128)} %get-tuple-element.19) | copy-start | bytes 1540
  110.9 65.8 %copy-start = (bf16[2,512,512]{2,1,0:T(8,128)(2,1)S(1)}, bf16[2,512,512]{2,1,0:T(8,128)(2,1)}, u32[]{:S(2)}) copy-start(bf16[2,512,512]{2,1,0:T(8,128)(2,1)} %param.17) | copy-start | bytes 3145732
  110.9 66.9 %copy-start.1 = (bf16[2,512,512]{2,1,0:T(8,128)(2,1)S(1)}, bf16[2,512,512]{2,1,0:T(8,128)(2,1)}, u32[]{:S(2)}) copy-start(bf16[2,512,512]{2,1,0:T(8,128)(2,1)} %param.18) | copy-start | bytes 3145732
  110.9 68.1 %copy-start.2 = (bf16[2,512,512]{2,1,0:T(8,128)(2,1)S(1)}, bf16[2,512,512]{2,1,0:T(8,128)(2,1)}, u32[]{:S(2)}) copy-start(bf16[2,512,512]{2,1,0:T(8,128)(2,1)} %param.19) | copy-start | bytes 3145732
  150.0 49.9 %reduce-scatter.23.cloned.1.call-start = ((), (), s32[]{:S(2)}) async-start(), calls=%async_computation.16 | async-start | bytes 655360 | tf_op jit(solution)/shard_map/reduce_scatter | solution.py:65
  177.8 44.5 %reduce-scatter.25.cloned.1.call-start = ((), (), s32[]{:S(2)}) async-start(), calls=%async_computation.17 | async-start | bytes 655360 | tf_op jit(solution)/shard_map/reduce_scatter | solution.py:65
  178.9 65.7 %reduce-scatter.27.cloned.1.call-start = ((), (), s32[]{:S(2)}) async-start(), calls=%async_computation.18 | async-start | bytes 655360 | tf_op jit(solution)/shard_map/reduce_scatter | solution.py:65
  180.1 86.9 %reduce-scatter.21.cloned.1.call-start = ((), (), s32[]{:S(2)}) async-start(), calls=%async_computation.15 | async-start | bytes 655360 | tf_op jit(solution)/shard_map/reduce_scatter | solution.py:65
  182.4 170.8 %reduce-scatter.29.cloned.1.call-start = ((), (), s32[]{:S(2)}) async-start(), calls=%async_computation.19 | async-start | bytes 655360 | tf_op jit(solution)/shard_map/reduce_scatter | solution.py:83
  291.8 22.8 %copy-start.9 = (f32[128]{0:T(128)S(1)}, f32[128]{0:T(128)}, u32[]{:S(2)}) copy-start(f32[128]{0:T(128)} %get-tuple-element.18) | copy-start | bytes 1540
  291.8 36.8 %copy-start.3 = (bf16[2,512,512]{2,1,0:T(8,128)(2,1)S(1)}, bf16[2,512,512]{2,1,0:T(8,128)(2,1)}, u32[]{:S(2)}) copy-start(bf16[2,512,512]{2,1,0:T(8,128)(2,1)} %param.20) | copy-start | bytes 3145732
Sparse Core Ops, SparseCore 0:
  17.7 23.1 reduce-scatter.12
  43.2 20.1 reduce-scatter.14
  65.6 20.1 reduce-scatter.16
  87.9 20.0 reduce-scatter.10
  150.1 19.8 reduce-scatter.18
  177.9 21.9 reduce-scatter.22
  202.2 20.0 reduce-scatter.24
  224.6 20.0 reduce-scatter.26
  247.0 20.0 reduce-scatter.20
  329.8 19.8 reduce-scatter.28
where the time goes:
time: 362 us
  waiting for transfers between devices  161 us (44%)
  blocking collectives  64.5 us (18%)
  matrix products  62.6 us (17%)
  other arithmetic  54.8 us (15%)
  between operations  14.5 us (4%)
  local copies, waits for them, and re-layouts  3.97 us (1%)
    reduce_scatter x8, waiting for transfers between devices, shards(): sums = lax.psum_scatter(terms, 'dp', scatter_dimension=0, tiled=True)  141 us
    dot_general x2, matrix products, advance(): jnp.einsum('bhk,bhkv->bhv', query.reshape(count, heads, size), updated, p...  45.3 us
    all_gather x2, blocking collectives, shards(): gathered = lax.all_gather(normed, 'dp', axis=0, tiled=True)  27.6 us
    psum x2, blocking collectives, shards(): squares_all = lax.psum(partial_sq, 'dp')  23.7 us
    another operation x1, other arithmetic, shards(): return (result, jnp.stack(states))  23.4 us
    add x1, other arithmetic, advance(): updated = forget[..., None] * prior + key[..., None] * values[:, :, None, :]  23.2 us
    reduce_scatter x2, waiting for transfers between devices, shards(): lax.psum_scatter(jnp.dot(gathered, out_weight, preferred_element_type=jnp...  19.9 us
    dot_general x8, matrix products, shards(): jnp.dot(gained, weight[block], preferred_element_type=jnp.float32)  14.1 us
  transfers between devices with their start and end apart: 10, of which 9 were waited for; matrix products, arithmetic and copies ran while one was open for 11% of the time, Pallas kernels for 0%

commit v1 on v0

--- a/solution.py
+++ b/solution.py
@@ -51,7 +51,12 @@
         whole = lax.all_gather(current, "tp", axis=0, tiled=True)
         whole_wide = whole.astype(jnp.float32)
         partial_sq = jnp.sum(whole_wide * whole_wide, axis=1)
-        squares_all = lax.psum(partial_sq, "dp")
+
+        def quarters_recast(incoming_x):
+            raw_out = lax.all_gather(incoming_x, axis_name="dp")
+            return jnp.sum(raw_out, axis=0)
+
+        squares_all = quarters_recast(partial_sq)
         squares = lax.dynamic_slice_in_dim(
             squares_all, lax.axis_index("dp") * own_count, own_count, 0
         )

time: 362 us -> 362 us (level)
    psum x2 -> x0, blocking collectives: 23.7 us -> none  [shards(): squares_all = lax.psum(partial_sq, 'dp')]
    all_gather x0 -> x2, blocking collectives: none -> 22.3 us  [quarters_recast(): raw_out = lax.all_gather(incoming_x, axis_name='dp')]
where the time goes in v1:
time: 362 us; the launch traced here: 361 us
  waiting for transfers between devices  162 us (45%)
  blocking collectives  63.2 us (17%)
  matrix products  62.6 us (17%)
  other arithmetic  54.9 us (15%)
  between operations  14.5 us (4%)
  local copies, waits for them, and re-layouts  3.97 us (1%)
    reduce_scatter x8, waiting for transfers between devices, shards(): sums = lax.psum_scatter(terms, 'dp', scatter_dimension=0, tiled=True)  142 us
    dot_general x2, matrix products, advance(): jnp.einsum('bhk,bhkv->bhv', query.reshape(count, heads, size), updated, p...  45.3 us
    all_gather x2, blocking collectives, shards(): gathered = lax.all_gather(normed, 'dp', axis=0, tiled=True)  27.7 us
    another operation x1, other arithmetic, shards(): return (result, jnp.stack(states))  23.4 us
    add x1, other arithmetic, advance(): updated = forget[..., None] * prior + key[..., None] * values[:, :, None, :]  23.2 us
    all_gather x2, blocking collectives, quarters_recast(): raw_out = lax.all_gather(incoming_x, axis_name='dp')  22.3 us
    reduce_scatter x2, waiting for transfers between devices, shards(): lax.psum_scatter(jnp.dot(gathered, out_weight, preferred_element_type=jnp...  19.8 us
    dot_general x8, matrix products, shards(): jnp.dot(gained, weight[block], preferred_element_type=jnp.float32)  14.1 us
  transfers between devices with their start and end apart: 10, of which 9 were waited for; matrix products, arithmetic and copies ran while one was open for 11% of the time, Pallas kernels for 0%

profile of v1, /device:TPU:0, one launch (start us, length us, event | category | flops | bytes accessed | tf_op | source)
XLA Modules:
  0.0 361.3 jit_solution(12222880513553631090)
XLA Ops:
  7.2 0.8 slice_convert_fusion
  8.0 7.4 %all_gather.24 = bf16[256,512]{1,0:T(8,128)(2,1)S(1)} all-gather(bf16[64,512]{1,0:T(8,128)(2,1)} %param.12), channel_id=1, replica_groups=mesh['grp'=2,'tp'=4,'dp'=4] {'tp'}, dimensions={0}, use_global_device_ids=true | all-gather | bytes 327680 | tf_op jit(solution)/shard_map/all_gather | solution.py:51
  15.4 2.1 fusion.36
  17.6 2.1 fusion.34
  19.8 2.2 fusion.32
  22.1 2.2 fusion.38
  24.3 0.1 fusion.16
  24.5 11.4 %all-gather.2 = f32[4,1,256]{2,1,0:T(1,128)S(1)} all-gather(f32[1,1,256]{2,1,0:T(1,128)S(1)} %bitcast.96), channel_id=2, replica_groups=mesh['grp'=2,'tp'=4,'dp'=4] {'dp'}, dimensions={0}, use_global_device_ids=true | all-gather | bytes 5120 | tf_op jit(solution)/shard_map/all_gather | solution.py:56
  35.8 0.1 add_rsqrt_fusion.3
  35.9 0.7 multiply_log_fusion
  36.6 1.3 slice_bitcast_fusion
  37.9 0.8 fusion.62
  38.7 0.8 broadcast_subtract_fusion
  39.5 1.3 reduce-scatter.13.cloned.1.call-done
  40.8 22.5 %reduce-scatter.15.cloned.1.call-done = f32[64,512]{1,0:T(8,128)} async-done(((f32[256,512]{1,0:T(8,128)}), f32[64,512]{1,0:T(8,128)}) %reduce-scatter.15.cloned.1.call-update) | async-done | bytes 131088 | tf_op jit(solution)/shard_map/reduce_scatter | solution.py:70
  63.3 22.4 %reduce-scatter.17.cloned.1.call-done = f32[64,512]{1,0:T(8,128)} async-done(((f32[256,512]{1,0:T(8,128)}), f32[64,512]{1,0:T(8,128)}) %reduce-scatter.17.cloned.1.call-update) | async-done | bytes 131088 | tf_op jit(solution)/shard_map/reduce_scatter | solution.py:70
  85.7 22.3 %reduce-scatter.11.cloned.1.call-done = f32[64,512]{1,0:T(8,128)} async-done(((f32[256,512]{1,0:T(8,128)}), f32[64,512]{1,0:T(8,128)}) %reduce-scatter.11.cloned.1.call-update) | async-done | bytes 131088 | tf_op jit(solution)/shard_map/reduce_scatter | solution.py:70
  108.0 1.2 multiply_add_fusion.3
  109.5 0.7 reshape.56
  110.2 0.7 reshape.69
  110.9 22.7 %fusion.4 = f32[64,4,1,128]{3,2,1,0:T(1,128)S(1)} fusion(f32[64,4,128,1]{2,3,1,0:T(1,128)} %bitcast.81, f32[2,64,4,128,128]{4,3,2,1,0:T(8,128)} %param.13, f32[64,4,128]{2,1,0:T(4,128)S(1)} %mul.316, f32[64,4,128]{2,1,0:T(4,128)S(1)} %mul.313, f32[64,4,128]{2,1,0:T(4,128)S(1)} %mul.309), kind=kOutput, calls=%fused_computation.6 | convolution fusion | flops 62914560 | bytes 17432576 | tf_op jit(solution)/shard_map/bhk,bhkv->bhv/dot_general | solution.py:22
  133.6 0.1 multiply_reduce_fusion.1
  133.8 0.1 fusion.61
  134.0 13.9 %all_gather.27 = bf16[256,512]{1,0:T(8,128)(2,1)S(1)} all-gather(bf16[64,512]{1,0:T(8,128)(2,1)S(1)} %bitcast.76), channel_id=1, replica_groups=mesh['grp'=2,'tp'=4,'dp'=4] {'dp'}, dimensions={0}, use_global_device_ids=true | all-gather | bytes 327680 | tf_op jit(solution)/shard_map/all_gather | solution.py:86
  147.8 2.1 fusion.30
  150.1 19.8 %reduce-scatter.19.cloned.1.call-done = f32[64,512]{1,0:T(8,128)} async-done(((f32[256,512]{1,0:T(8,128)}), f32[64,512]{1,0:T(8,128)}) %reduce-scatter.19.cloned.1.call-update) | async-done | bytes 131088 | tf_op jit(solution)/shard_map/reduce_scatter | solution.py:88
  169.9 0.9 add_convert_fusion
  170.8 5.8 %all_gather.28 = bf16[256,512]{1,0:T(8,128)(2,1)S(1)} all-gather(bf16[64,512]{1,0:T(8,128)(2,1)S(1)} %add_convert_fusion), channel_id=1, replica_groups=mesh['grp'=2,'tp'=4,'dp'=4] {'tp'}, dimensions={0}, use_global_device_ids=true | all-gather | bytes 327680 | tf_op jit(solution)/shard_map/all_gather | solution.py:51
  176.6 1.1 fusion.26
  177.8 1.1 fusion.24
  178.9 1.1 fusion.22
  180.1 2.2 fusion.28
  182.4 0.1 fusion.18
  182.5 10.9 %all-gather.3 = f32[4,1,256]{2,1,0:T(1,128)S(1)} all-gather(f32[1,1,256]{2,1,0:T(1,128)S(1)} %bitcast.97), channel_id=3, replica_groups=mesh['grp'=2,'tp'=4,'dp'=4] {'dp'}, dimensions={0}, use_global_device_ids=true | all-gather | bytes 5120 | tf_op jit(solution)/shard_map/all_gather | solution.py:56
  193.5 0.1 add_rsqrt_fusion.2
  193.5 6.2 %reduce-scatter.23.cloned.1.call-done = f32[64,512]{1,0:T(8,128)} async-done(((f32[256,512]{1,0:T(8,128)}), f32[64,512]{1,0:T(8,128)}) %reduce-scatter.23.cloned.1.call-update) | async-done | bytes 131088 | tf_op jit(solution)/shard_map/reduce_scatter | solution.py:70
  199.7 22.3 %reduce-scatter.25.cloned.1.call-done = f32[64,512]{1,0:T(8,128)} async-done(((f32[256,512]{1,0:T(8,128)}), f32[64,512]{1,0:T(8,128)}) %reduce-scatter.25.cloned.1.call-update) | async-done | bytes 131088 | tf_op jit(solution)/shard_map/reduce_scatter | solution.py:70
  222.1 22.4 %reduce-scatter.27.cloned.1.call-done = f32[64,512]{1,0:T(8,128)} async-done(((f32[256,512]{1,0:T(8,128)}), f32[64,512]{1,0:T(8,128)}) %reduce-scatter.27.cloned.1.call-update) | async-done | bytes 131088 | tf_op jit(solution)/shard_map/reduce_scatter | solution.py:70
  244.4 22.4 %reduce-scatter.21.cloned.1.call-done = f32[64,512]{1,0:T(8,128)} async-done(((f32[256,512]{1,0:T(8,128)}), f32[64,512]{1,0:T(8,128)}) %reduce-scatter.21.cloned.1.call-update) | async-done | bytes 131088 | tf_op jit(solution)/shard_map/reduce_scatter | solution.py:70
  266.8 1.3 multiply_add_fusion.2
  268.4 23.2 %multiply_add_fusion.1 = (f32[1,64,4,128,128]{4,3,2,1,0:T(8,128)}, f32[1,64,4,128,128]{4,3,2,1,0:T(8,128)}) fusion(f32[2,64,4,128,128]{4,3,2,1,0:T(8,128)} %param.13, f32[64,4,128]{2,1,0:T(4,128)} %copy-done.6, f32[64,4,128]{2,1,0:T(4,128)} %copy-done.5, f32[64,4,128]{2,1,0:T(4,128)} %copy-done.4, f32[64,4,128]{2,1,0:T(4,128)S(1)} %mul.349, ...), kind=kLoop, calls=%fused_computation.8 | loop fusion | flops 25165824 | bytes 67895296 | tf_op jit(solution)/shard_map/add | solution.py:21
  291.6 22.6 %fusion.1 = f32[64,4,1,128]{3,2,1,0:T(1,128)S(1)} fusion(f32[64,4,128,1]{2,3,1,0:T(1,128)S(1)} %bitcast.80, f32[2,64,4,128,128]{4,3,2,1,0:T(8,128)} %param.13, f32[64,4,128]{2,1,0:T(4,128)S(1)} %mul.349, f32[64,4,128]{2,1,0:T(4,128)S(1)} %mul.346, f32[64,4,128]{2,1,0:T(4,128)S(1)} %mul.342), kind=kOutput, calls=%fused_computation.3 | convolution fusion | flops 62914560 | bytes 17432576 | tf_op jit(solution)/shard_map/bhk,bhkv->bhv/dot_general | solution.py:22
  314.2 0.1 multiply_reduce_fusion
  314.4 0.1 fusion.60
  314.6 13.8 %all_gather.31 = bf16[256,512]{1,0:T(8,128)(2,1)S(1)} all-gather(bf16[64,512]{1,0:T(8,128)(2,1)S(1)} %bitcast.77), channel_id=1, replica_groups=mesh['grp'=2,'tp'=4,'dp'=4] {'dp'}, dimensions={0}, use_global_device_ids=true | all-gather | bytes 327680 | tf_op jit(solution)/shard_map/all_gather | solution.py:86
  328.4 1.1 fusion.20
  329.5 23.4 %pad_maximum_fusion = f32[2,64,4,128,128]{4,3,2,1,0:T(8,128)} fusion(f32[1,64,4,128,128]{4,3,2,1,0:T(8,128)} %get-tuple-element.7, f32[1,64,4,128,128]{4,3,2,1,0:T(8,128)} %get-tuple-element.6), kind=kLoop, calls=%fused_computation | loop fusion | flops 8388608 | bytes 67108864 | tf_op jit(solution)/shard_map/stack | solution.py:98
  352.9 1.6 convert_add_fusion
  (57 shorter events, 1.1 us)
Async XLA Ops:
  7.2 33.6 %reduce-scatter.13.cloned.1.call-start = ((), (), s32[]{:S(2)}) async-start(), calls=%async_computation.11 | async-start | bytes 655360 | tf_op jit(solution)/shard_map/reduce_scatter | solution.py:70
  17.6 45.7 %reduce-scatter.15.cloned.1.call-start = ((), (), s32[]{:S(2)}) async-start(), calls=%async_computation.12 | async-start | bytes 655360 | tf_op jit(solution)/shard_map/reduce_scatter | solution.py:70
  19.8 65.9 %reduce-scatter.17.cloned.1.call-start = ((), (), s32[]{:S(2)}) async-start(), calls=%async_computation.13 | async-start | bytes 655360 | tf_op jit(solution)/shard_map/reduce_scatter | solution.py:70
  22.0 86.0 %reduce-scatter.11.cloned.1.call-start = ((), (), s32[]{:S(2)}) async-start(), calls=%async_computation.10 | async-start | bytes 655360 | tf_op jit(solution)/shard_map/reduce_scatter | solution.py:70
  24.3 145.6 %reduce-scatter.19.cloned.1.call-start = ((), (), s32[]{:S(2)}) async-start(), calls=%async_computation.14 | async-start | bytes 655360 | tf_op jit(solution)/shard_map/reduce_scatter | solution.py:88
  36.6 74.3 %copy-start.8 = (f32[64]{0:T(128)}, f32[64]{0:T(128)S(1)}, u32[]{:S(2)}) copy-start(f32[64]{0:T(128)S(1)} %multiply_log_fusion) | copy-start | bytes 772
  109.3 24.6 %copy-start.4 = (f32[64,4,128]{2,1,0:T(4,128)}, f32[64,4,128]{2,1,0:T(4,128)S(1)}, u32[]{:S(2)}) copy-start(f32[64,4,128]{2,1,0:T(4,128)S(1)} %mul.309) | copy-start | bytes 393220
  109.4 24.6 %copy-start.5 = (f32[64,4,128]{2,1,0:T(4,128)}, f32[64,4,128]{2,1,0:T(4,128)S(1)}, u32[]{:S(2)}) copy-start(f32[64,4,128]{2,1,0:T(4,128)S(1)} %mul.313) | copy-start | bytes 393220
  109.4 40.6 %copy-start.6 = (f32[64,4,128]{2,1,0:T(4,128)}, f32[64,4,128]{2,1,0:T(4,128)S(1)}, u32[]{:S(2)}) copy-start(f32[64,4,128]{2,1,0:T(4,128)S(1)} %mul.316) | copy-start | bytes 393220
  110.9 22.9 %copy-start.7 = (f32[64,4,128]{2,1,0:T(4,128)S(1)}, f32[64,4,128]{2,1,0:T(4,128)}, u32[]{:S(2)}) copy-start(f32[64,4,128]{2,1,0:T(4,128)} %reshape.56) | copy-start | bytes 393220
  110.9 22.9 %copy-start.10 = (f32[128]{0:T(128)S(1)}, f32[128]{0:T(128)}, u32[]{:S(2)}) copy-start(f32[128]{0:T(128)} %get-tuple-element.19) | copy-start | bytes 1540
  110.9 65.7 %copy-start = (bf16[2,512,512]{2,1,0:T(8,128)(2,1)S(1)}, bf16[2,512,512]{2,1,0:T(8,128)(2,1)}, u32[]{:S(2)}) copy-start(bf16[2,512,512]{2,1,0:T(8,128)(2,1)} %param.17) | copy-start | bytes 3145732
  110.9 66.9 %copy-start.1 = (bf16[2,512,512]{2,1,0:T(8,128)(2,1)S(1)}, bf16[2,512,512]{2,1,0:T(8,128)(2,1)}, u32[]{:S(2)}) copy-start(bf16[2,512,512]{2,1,0:T(8,128)(2,1)} %param.18) | copy-start | bytes 3145732
  110.9 68.1 %copy-start.2 = (bf16[2,512,512]{2,1,0:T(8,128)(2,1)S(1)}, bf16[2,512,512]{2,1,0:T(8,128)(2,1)}, u32[]{:S(2)}) copy-start(bf16[2,512,512]{2,1,0:T(8,128)(2,1)} %param.19) | copy-start | bytes 3145732
  150.0 49.7 %reduce-scatter.23.cloned.1.call-start = ((), (), s32[]{:S(2)}) async-start(), calls=%async_computation.16 | async-start | bytes 655360 | tf_op jit(solution)/shard_map/reduce_scatter | solution.py:70
  177.7 44.3 %reduce-scatter.25.cloned.1.call-start = ((), (), s32[]{:S(2)}) async-start(), calls=%async_computation.17 | async-start | bytes 655360 | tf_op jit(solution)/shard_map/reduce_scatter | solution.py:70
  178.9 65.6 %reduce-scatter.27.cloned.1.call-start = ((), (), s32[]{:S(2)}) async-start(), calls=%async_computation.18 | async-start | bytes 655360 | tf_op jit(solution)/shard_map/reduce_scatter | solution.py:70
  180.1 86.8 %reduce-scatter.21.cloned.1.call-start = ((), (), s32[]{:S(2)}) async-start(), calls=%async_computation.15 | async-start | bytes 655360 | tf_op jit(solution)/shard_map/reduce_scatter | solution.py:70
  182.3 170.6 %reduce-scatter.29.cloned.1.call-start = ((), (), s32[]{:S(2)}) async-start(), calls=%async_computation.19 | async-start | bytes 655360 | tf_op jit(solution)/shard_map/reduce_scatter | solution.py:88
  291.6 22.8 %copy-start.9 = (f32[128]{0:T(128)S(1)}, f32[128]{0:T(128)}, u32[]{:S(2)}) copy-start(f32[128]{0:T(128)} %get-tuple-element.18) | copy-start | bytes 1540
  291.6 36.8 %copy-start.3 = (bf16[2,512,512]{2,1,0:T(8,128)(2,1)S(1)}, bf16[2,512,512]{2,1,0:T(8,128)(2,1)}, u32[]{:S(2)}) copy-start(bf16[2,512,512]{2,1,0:T(8,128)(2,1)} %param.20) | copy-start | bytes 3145732
Sparse Core Ops, SparseCore 0:
  17.7 23.0 reduce-scatter.12
  43.0 20.2 reduce-scatter.14
  65.6 20.1 reduce-scatter.16
  87.9 20.1 reduce-scatter.10
  150.1 19.7 reduce-scatter.18
  177.8 21.8 reduce-scatter.22
  202.0 20.0 reduce-scatter.24
  224.3 20.0 reduce-scatter.26
  246.7 20.0 reduce-scatter.20
  329.6 19.8 reduce-scatter.28
